TPU v7x, 128 devices: a whole 4x4x4 slice. The times are simulated.
128 devices in a mesh: ep: 64 (over z, y, x), tp: 2 (over core).
Axes of the slice: x: 4, y: 4, z: 4, core: 2. Of those that a mesh axis runs over, the one named last changes fastest.
Arguments:
- inputs: bfloat16 [1024, 2048], P('ep'), may hold values from -6 to 6
- positions: int32 [1024], P('ep'), may hold values from 1024 to 8191
- ret_state: float32 [1024, 12, 128, 128], P('ep', 'tp'), may hold values from -4 to 4
- norm_mix: bfloat16 [2048], replicated, may hold values from 0.099609375 to 1.8984375
- w_query: bfloat16 [2048, 1536], P('ep', 'tp'), may hold values from -0.375 to 0.375
- w_key: bfloat16 [2048, 1536], P('ep', 'tp'), may hold values from -0.375 to 0.375
- w_value: bfloat16 [2048, 1536], P('ep', 'tp'), may hold values from -0.375 to 0.375
- w_gate_in: bfloat16 [2048, 1536], P('ep', 'tp'), may hold values from -0.375 to 0.375
- head_gain: bfloat16 [1536], P('tp'), may hold values from 0.099609375 to 1.8984375
- w_out: bfloat16 [1536, 2048], P('tp', 'ep'), may hold values from -0.15625 to 0.15625
- norm_ffn: bfloat16 [2048], replicated, may hold values from 0.099609375 to 1.8984375
- route_ids: int32 [1024, 4], P('ep'), may hold values from 0 to 63, all different within a row; in each aligned block of 16 rows (0 to 15, 16 to 31, ...) at most 2 rows name the same one
- route_weight: bfloat16 [1024, 4], P('ep'), may hold values from 0.19921875 to 1
- exp_gate: bfloat16 [64, 2048, 1024], P('ep', None, 'tp'), may hold values from -0.125 to 0.125
- exp_up: bfloat16 [64, 2048, 1024], P('ep', None, 'tp'), may hold values from -0.125 to 0.125
- exp_down: bfloat16 [64, 1024, 2048], P('ep', 'tp'), may hold values from -0.1875 to 0.1875
- dense_gate: bfloat16 [2048, 4096], P(None, ('ep', 'tp')), may hold values from -0.125 to 0.125
- dense_up: bfloat16 [2048, 4096], P(None, ('ep', 'tp')), may hold values from -0.125 to 0.125
- dense_down: bfloat16 [4096, 2048], P(('ep', 'tp')), may hold values from -0.375 to 0.375
- branch_gate: bfloat16 [2048], replicated, may hold values from -0.125 to 0.125
Outputs:
- layer_out: bfloat16 [1024, 2048], P('ep')
- new_state: float32 [1024, 12, 128, 128], P('ep', 'tp')
Inputs may be any that keep to these rules, and one draw needn't show every extreme that they name: `route_ids`: each row names 4 different experts. Among the rows of one index of ep no expert is named more than 2 times, a bound that some block reaches.
All inputs are finite; a program needn't handle non-finite values.
Results may differ from a plain program's by a relative error of at most 0.015.
Values may be sent and summed in bfloat16 or wider, within the bound.
No kernel may reach another device: no remote copies, remote signals or barrier semaphores. Data moves between devices by JAX's collectives and lax.ppermute only.
A program may use at most 128 MiB of HBM per device.

v0:
```python
import jax
import jax.numpy as jnp
from jax import lax
from jax.sharding import PartitionSpec as P

D = 2048
HEADS = 12
EPS = 1e-06


def in_one_piece(arrays, axis, dim, along):
    both = jnp.concatenate(arrays, axis=along)
    out, at, done = (lax.all_gather(both, axis, axis=dim, tiled=True), 0, [])
    for a in arrays:
        done.append(lax.slice_in_dim(out, at, at + a.shape[along], axis=along))
        at += a.shape[along]
    return tuple(done)


def sent_to_all(array, axis):
    copies = jnp.broadcast_to(array, (lax.axis_size(axis), *array.shape))
    return lax.all_to_all(copies, axis, split_axis=0, concat_axis=0, tiled=True)


def over_copies(array, axis):
    everything = sent_to_all(array, axis)
    return jnp.sum(everything.astype(jnp.float32), axis=0)


def split_up(array, dim, size):
    before, after = (array.shape[:dim], array.shape[dim + 1 :])
    return jnp.moveaxis(array.reshape(*before, size, -1, *after), dim, 0)


def summed_on_arrival(array, axis, dim):
    size = lax.axis_size(axis)
    tiles = lax.all_to_all(split_up(array, dim, size), axis, 0, 0, tiled=True)
    return jnp.sum(tiles.astype(jnp.float32), axis=0)


def rms_scale(values, scales):
    widened = values.astype(jnp.float32)
    scaled = widened * lax.rsqrt(jnp.mean(widened * widened, axis=-1, keepdims=True) + EPS)
    return (scaled * scales.astype(jnp.float32)).astype(jnp.bfloat16)


def rotary_angles(positions, head_dim):
    halfway = head_dim // 2
    frequency = 10000.0 ** (-jnp.arange(halfway, dtype=jnp.float32) * 2.0 / head_dim)
    return positions.astype(jnp.float32)[:, None] * frequency[None, :]


def rotate_heads(values, angles):
    halfway = values.shape[-1] // 2
    cosine = jnp.cos(angles)[:, None, :]
    sine_of = jnp.sin(angles)[:, None, :]
    leading = values[..., :halfway]
    trailing = values[..., halfway:]
    return jnp.concatenate(
        [leading * cosine - trailing * sine_of, trailing * cosine + leading * sine_of], axis=-1
    )


def log_decay(head_count):
    spread = jnp.arange(head_count, dtype=jnp.float32) * (5.0 / max(head_count - 1, 1))
    return jnp.log1p(-(2.0 ** (-5.0 - spread)))


def retain(queries, keys_in, values_in, gate_pre, old_state, positions, scales, log_gamma):
    row_count, head_count, head_dim = (old_state.shape[0], old_state.shape[1], old_state.shape[2])
    angles = rotary_angles(positions, head_dim)
    rot_query = rotate_heads(
        queries.astype(jnp.float32).reshape(row_count, head_count, head_dim), angles
    )
    rot_key = rotate_heads(
        keys_in.astype(jnp.float32).reshape(row_count, head_count, head_dim), angles
    ) * head_dim ** (-0.5)
    value_heads = values_in.astype(jnp.float32).reshape(row_count, head_count, head_dim)
    new_state = (
        jnp.exp(log_gamma)[None, :, None, None] * old_state
        + rot_key[:, :, :, None] * value_heads[:, :, None, :]
    )
    readout = jnp.einsum("shd,shdv->shv", rot_query, new_state, precision=lax.Precision.HIGHEST)
    centred = readout - jnp.mean(readout, axis=-1, keepdims=True)
    normed = centred * lax.rsqrt(jnp.mean(centred * centred, axis=-1, keepdims=True) + EPS)
    normed = normed * scales.astype(jnp.float32).reshape(head_count, head_dim)
    gated_out = normed.reshape(row_count, head_count * head_dim) * jax.nn.silu(
        gate_pre.astype(jnp.float32)
    )
    return (gated_out.astype(jnp.bfloat16), new_state)


def slot_of(route_ids, expert_count, capacity):
    flat_ids = route_ids.reshape(-1)
    onehot = (flat_ids[:, None] == jnp.arange(expert_count, dtype=jnp.int32)[None, :]).astype(
        jnp.int32
    )
    ranking = jnp.sum((jnp.cumsum(onehot, axis=0) - 1) * onehot, axis=1)
    return flat_ids * capacity + ranking


def on_device(
    inputs,
    positions,
    ret_state,
    norm_mix,
    w_query,
    w_key,
    w_value,
    w_gate_in,
    head_gain,
    w_out,
    norm_ffn,
    route_ids,
    route_weight,
    exp_gate,
    exp_up,
    exp_down,
    dense_gate,
    dense_up,
    dense_down,
    branch_gate,
):
    seq_count = inputs.shape[0]
    top_count = route_ids.shape[1]
    ep_size = lax.axis_size("ep")
    local_experts = exp_gate.shape[0]
    expert_count = ep_size * local_experts
    capacity = max(2, 2 * seq_count * top_count // expert_count)
    normed = rms_scale(inputs, norm_mix)
    segments = in_one_piece((w_query, w_key, w_value, w_gate_in), "ep", 0, 1)
    totals = tuple(
        (
            jnp.dot(normed, weight_rows, preferred_element_type=jnp.float32)
            for weight_rows in segments
        )
    )
    queries, keys_new, values_new, gate_pre = [member.astype(jnp.bfloat16) for member in totals]
    local_heads = ret_state.shape[1]
    log_gamma = lax.dynamic_slice_in_dim(
        log_decay(HEADS), lax.axis_index("tp") * local_heads, local_heads
    )
    retained, new_state = retain(
        queries, keys_new, values_new, gate_pre, ret_state, positions, head_gain, log_gamma
    )
    partial_rows = jnp.dot(
        retained,
        lax.all_gather(w_out, "ep", axis=1, tiled=True),
        preferred_element_type=jnp.float32,
    )
    rounded = lax.optimization_barrier(partial_rows.astype(jnp.bfloat16)).astype(jnp.float32)
    mixer_out = (
        over_copies(rounded.astype(jnp.bfloat16), "tp").astype(jnp.float32).astype(jnp.bfloat16)
    )
    residual_sum = (inputs.astype(jnp.float32) + mixer_out.astype(jnp.float32)).astype(jnp.bfloat16)
    normed_ffn = rms_scale(residual_sum, norm_ffn)
    slot_index = slot_of(route_ids, expert_count, capacity)
    slot_total = expert_count * capacity
    placing = (jnp.arange(slot_total, dtype=jnp.int32)[:, None] == slot_index[None, :]).astype(
        jnp.float32
    )
    by_token = jnp.sum(placing.reshape(slot_total, seq_count, top_count), axis=2)
    outgoing = (
        jnp.dot(by_token.astype(jnp.bfloat16), normed_ffn, preferred_element_type=jnp.float32)
        .astype(jnp.bfloat16)
        .reshape(expert_count, capacity, D)
    )
    received = lax.all_to_all(outgoing, "ep", split_axis=0, concat_axis=0, tiled=True)
    slot_count = received.shape[1]
    grouped = received.reshape(ep_size, local_experts, slot_count, D)
    gate_part = jnp.einsum("sjnd,jdf->sjnf", grouped, exp_gate, preferred_element_type=jnp.float32)
    up_part = jnp.einsum("sjnd,jdf->sjnf", grouped, exp_up, preferred_element_type=jnp.float32)
    hidden = (jax.nn.silu(gate_part) * up_part).astype(jnp.bfloat16)
    partial_out = jnp.einsum(
        "sjnf,jfd->sjnd", hidden, exp_down, preferred_element_type=jnp.float32
    ).reshape(received.shape[0], slot_count, D)
    returned = lax.all_to_all(
        partial_out.astype(jnp.bfloat16), "ep", split_axis=0, concat_axis=0, tiled=True
    ).astype(partial_out.dtype)
    widened = route_weight.astype(jnp.float32)
    share_flat = (widened / jnp.sum(widened, axis=-1, keepdims=True)).reshape(-1)
    weighting = jnp.sum(
        (placing * share_flat[None, :]).reshape(slot_total, seq_count, top_count), axis=2
    )
    expert_part = jnp.einsum(
        "rt,rd->td", weighting, returned.reshape(slot_total, D), precision=lax.Precision.HIGHEST
    )
    segment = lax.all_gather(normed_ffn, "ep", axis=0, tiled=True)
    gate_part = jnp.dot(segment, dense_gate, preferred_element_type=jnp.float32)
    up_part = jnp.dot(segment, dense_up, preferred_element_type=jnp.float32)
    hidden = (jax.nn.silu(gate_part) * up_part).astype(jnp.bfloat16)
    opening = jax.nn.sigmoid(
        jnp.dot(segment, branch_gate[:, None], preferred_element_type=jnp.float32)
    )
    branch_term = jnp.dot(hidden, dense_down, preferred_element_type=jnp.float32) * opening
    summed_branch = summed_on_arrival(branch_term.astype(jnp.bfloat16), "ep", 0)
    summed_branch = summed_branch + expert_part
    width_total = over_copies(summed_branch.astype(jnp.bfloat16), "tp").astype(jnp.float32)
    layer_out = (residual_sum.astype(jnp.float32) + width_total).astype(jnp.bfloat16)
    return (layer_out, new_state)


def solution(mesh):
    in_specs = (
        P("ep", None),
        P("ep"),
        P("ep", "tp", None, None),
        P(),
        P("ep", "tp"),
        P("ep", "tp"),
        P("ep", "tp"),
        P("ep", "tp"),
        P("tp"),
        P("tp", "ep"),
        P(),
        P("ep", None),
        P("ep", None),
        P("ep", None, "tp"),
        P("ep", None, "tp"),
        P("ep", "tp", None),
        P(None, ("ep", "tp")),
        P(None, ("ep", "tp")),
        P(("ep", "tp"), None),
        P(),
    )
    out_specs = (P("ep", None), P("ep", "tp", None, None))
    return jax.shard_map(
        on_device, mesh=mesh, in_specs=in_specs, out_specs=out_specs, check_vma=False
    )
```

profile of v0, /device:TPU:1, one launch (start us, length us, event | category | flops | bytes accessed | tf_op | source)
XLA Modules:
  0.0 340.6 jit_solution(12423903585357650774)
XLA Ops:
  7.2 1.7 pad_maximum_fusion
  9.0 0.7 all-gather.6.cloned.1.call-update
  9.8 0.7 convert_element_type.100
  10.5 0.7 convert_element_type.103
  11.1 0.7 convert_element_type.113
  11.9 1.0 fusion.64
  12.9 0.7 bitcast_convert_fusion
  13.6 0.1 multiply_cosine_fusion
  13.7 91.6 %all-gather.4.cloned.1.call-done = bf16[2048,3072]{1,0:T(8,128)(2,1)} async-done(((bf16[32,3072]{1,0:T(8,128)(2,1)}), bf16[2048,3072]{1,0:T(8,128)(2,1)}) %all-gather.4.cloned.1.call-update) | async-done | bytes 12582928 | tf_op jit(solution)/shard_map/all_gather | solution.py:13
  105.3 2.5 fusion.33
  107.8 2.5 fusion.39
  110.4 2.4 fusion.45
  112.8 0.1 multiply_subtract_fusion.1
  112.9 0.1 maximum_multiply_fusion
  113.1 4.5 %multiply_add_fusion = f32[16,6,128,128]{3,2,1,0:T(8,128)S(1)} fusion(f32[16,6,128,128]{3,2,1,0:T(8,128)} %param.22, f32[16,6,128]{2,1,0:T(8,128)S(1)} %reshape.207, f32[16,6,128]{2,1,0:T(8,128)S(1)} %maximum_multiply_fusion, f32[6]{0:T(128)S(1)} %dynamic-slice_exponential_fusion), kind=kLoop, calls=%fused_computation.2 | loop fusion | flops 4718592 | bytes 12681240 | tf_op jit(solution)/shard_map/add | solution.py:80
  117.6 2.7 copy-done.2
  120.3 5.5 %fusion.84 = f32[16,6,1,128]{3,2,1,0:T(1,128)S(1)} fusion(f32[16,6,128,128]{3,2,1,0:T(8,128)S(1)} %multiply_add_fusion, f32[16,6,128,1]{2,1,0,3:T(8,128)S(1)} %maximum_bitcast_fusion), kind=kOutput, calls=%fused_computation.80 | convolution fusion | flops 18874368 | bytes 6389760 | tf_op jit(solution)/shard_map/shd,shdv->shv/dot_general | solution.py:83
  125.8 0.1 bitcast_reduce_fusion
  125.9 0.2 fusion.80
  126.0 0.1 fusion.81
  126.2 47.2 %all-gather.6.cloned.1.call-done = bf16[768,2048]{0,1:T(8,128)(2,1)} async-done(((bf16[768,32]{0,1:T(8,128)(2,1)}), bf16[768,2048]{0,1:T(8,128)(2,1)}) %all-gather.6.cloned.1.call-update) | async-done | bytes 3145744 | tf_op jit(solution)/shard_map/all_gather | solution.py:148
  173.4 4.5 %convolution_convert_fusion.2 = bf16[16,2048]{1,0:T(8,128)(2,1)S(1)} fusion(bf16[768,2048]{0,1:T(8,128)(2,1)} %all-gather.6.cloned.1.call-done, f32[2,8,6,128]{3,2,1,0:T(8,128)S(1)} %bitcast.87, bf16[2048,3072]{1,0:T(8,128)(2,1)} %all-gather.4.cloned.1.call-done, bf16[16,2048]{1,0:T(8,128)(2,1)S(1)} %copy-done.3, f32[2048]{0:T(1024)S(1)} %convert_element_type.100, ...), kind=kOutput, calls=%fused_computation.15 | convolution fusion | flops 100925440 | bytes 6479936 | tf_op jit(solution)/shard_map/dot_general | solution.py:146
  177.9 5.7 %all_to_all.25 = bf16[2,16,2048]{2,1,0:T(8,128)(2,1)S(1)} all-to-all(bf16[2,16,2048]{2,1,0:T(8,128)(2,1)S(1)} %broadcast_in_dim.4), channel_id=1, replica_groups=mesh['ep'=64,'tp'=2] {'tp'}, dimensions={0} | all-to-all | bytes 262144 | tf_op jit(solution)/shard_map/all_to_all | solution.py:22
  183.6 0.1 fusion.68
  183.8 0.7 fusion.70
  184.6 0.1 eq.31
  184.8 0.1 reduce_window_sum.11
  184.9 0.2 select_reduce_fusion.1
  185.1 0.1 copy.44
  185.4 1.2 convolution_convert_fusion.1
  186.5 1.1 reshape.197
  187.7 6.1 %all-to-all-start.2 = ((bf16[64,2,2048]{2,1,0:T(2,128)(2,1)}), bf16[64,2,2048]{2,1,0:T(2,128)(2,1)S(1)}, u32[]{:S(2)}, u32[]{:S(2)}) async-start(bf16[64,2,2048]{2,1,0:T(2,128)(2,1)} %reshape.197), calls=%async_computation.2 | async-start | bytes 1048576 | tf_op jit(solution)/shard_map/all_to_all | solution.py:168
  193.8 12.9 %all-to-all-done.2 = bf16[64,2,2048]{2,1,0:T(2,128)(2,1)S(1)} async-done(((bf16[64,2,2048]{2,1,0:T(2,128)(2,1)}), bf16[64,2,2048]{2,1,0:T(2,128)(2,1)S(1)}, u32[]{:S(2)}, u32[]{:S(2)}) %all-to-all-start.2) | async-done | bytes 524320 | tf_op jit(solution)/shard_map/all_to_all | solution.py:168
  206.7 2.0 fusion.14
  208.8 2.4 convolution_convert_fusion
  211.2 1.4 copy.47
  212.6 4.8 %all-to-all-start.3 = ((bf16[64,2,2048]{2,1,0:T(2,128)(2,1)}), bf16[64,2,2048]{2,1,0:T(2,128)(2,1)S(1)}, u32[]{:S(2)}, u32[]{:S(2)}) async-start(bf16[64,2,2048]{2,1,0:T(2,128)(2,1)} %copy.47), calls=%async_computation.3 | async-start | bytes 1048576 | tf_op jit(solution)/shard_map/all_to_all | solution.py:177
  217.5 36.3 %all-gather.8.cloned.1.call-done = bf16[1024,2048]{1,0:T(8,128)(2,1)} async-done(((bf16[16,2048]{1,0:T(8,128)(2,1)}), bf16[1024,2048]{1,0:T(8,128)(2,1)}) %all-gather.8.cloned.1.call-update) | async-done | bytes 4194320 | tf_op jit(solution)/shard_map/all_gather | solution.py:188
  253.8 3.7 %fusion.101 = f32[1024,32]{0,1:T(8,128)S(1)} fusion(bf16[1024,2048]{1,0:T(8,128)(2,1)} %all-gather.8.cloned.1.call-done, bf16[2048,32]{0,1:T(8,128)(2,1)} %param.36), kind=kOutput, calls=%fused_computation.107 | convolution fusion | flops 134217728 | bytes 4456448 | tf_op jit(solution)/shard_map/dot_general | solution.py:189
  257.5 1.2 fusion.102
  258.7 6.7 %multiply_convert_fusion = bf16[1024,2048]{1,0:T(8,128)(2,1)} fusion(bf16[32,2048]{1,0:T(8,128)(2,1)S(1)} %copy-done.4, f32[1024]{0:T(1024)S(1)} %add_divide_fusion, bf16[1024,2048]{1,0:T(8,128)(2,1)} %all-gather.8.cloned.1.call-done, bf16[2048,32]{0,1:T(8,128)(2,1)S(1)} %copy-done.5, f32[1024,32]{0,1:T(8,128)S(1)} %fusion.101), kind=kOutput, calls=%fused_computation.1 | convolution fusion | flops 272826368 | bytes 8785920 | tf_op jit(solution)/shard_map/dot_general | solution.py:195
  265.4 6.8 %all-to-all-start.1 = ((bf16[64,16,2048]{2,1,0:T(8,128)(2,1)}), bf16[64,16,2048]{2,1,0:T(8,128)(2,1)}, u32[]{:S(2)}, u32[]{:S(2)}) async-start(bf16[64,16,2048]{2,1,0:T(8,128)(2,1)} %bitcast.86), calls=%async_computation.1 | async-start | bytes 8388608 | tf_op jit(solution)/shard_map/all_to_all | solution.py:37
  272.2 0.2 reshape.202
  272.4 50.4 %all-to-all-done.1 = bf16[64,16,2048]{2,1,0:T(8,128)(2,1)} async-done(((bf16[64,16,2048]{2,1,0:T(8,128)(2,1)}), bf16[64,16,2048]{2,1,0:T(8,128)(2,1)}, u32[]{:S(2)}, u32[]{:S(2)}) %all-to-all-start.1) | async-done | bytes 4194336 | tf_op jit(solution)/shard_map/all_to_all | solution.py:37
  322.8 2.9 convert_reduce_fusion
  325.6 0.3 fusion.8
  326.0 7.5 %all_to_all.26 = bf16[2,16,2048]{2,1,0:T(8,128)(2,1)S(1)} all-to-all(bf16[2,16,2048]{2,1,0:T(8,128)(2,1)S(1)} %broadcast_in_dim.5), channel_id=1, replica_groups=mesh['ep'=64,'tp'=2] {'tp'}, dimensions={0} | all-to-all | bytes 262144 | tf_op jit(solution)/shard_map/all_to_all | solution.py:22
  333.4 0.7 fusion.71
  (47 shorter events, 0.9 us)
Async XLA Ops:
  7.2 201.6 %copy-start = (bf16[1,512,2048]{2,1,0:T(8,128)(2,1)S(1)}, bf16[1,512,2048]{2,1,0:T(8,128)(2,1)}, u32[]{:S(2)}) copy-start(bf16[1,512,2048]{2,1,0:T(8,128)(2,1)} %param.35) | copy-start | bytes 6291460
  7.2 103.2 %copy-start.3 = (bf16[16,2048]{1,0:T(8,128)(2,1)S(1)}, bf16[16,2048]{1,0:T(8,128)(2,1)}, u32[]{:S(2)}) copy-start(bf16[16,2048]{1,0:T(8,128)(2,1)} %param.20) | copy-start | bytes 196612
  7.2 98.1 %all-gather.4.cloned.1.call-start = ((), (), s32[]{:S(2)}) async-start(), calls=%async_computation.5 | async-start | bytes 12779520 | tf_op jit(solution)/shard_map/all_gather | solution.py:13
  9.0 164.4 %all-gather.6.cloned.1.call-start = ((), (), s32[]{:S(2)}) async-start(), calls=%async_computation.6 | async-start | bytes 3194880 | tf_op jit(solution)/shard_map/all_gather | solution.py:148
  9.7 244.0 %all-gather.8.cloned.1.call-start = ((), (), s32[]{:S(2)}) async-start(), calls=%async_computation.7 | async-start | bytes 4259840 | tf_op jit(solution)/shard_map/all_gather | solution.py:188
  117.6 2.7 copy-start.2
  125.7 58.8 %copy-start.6 = (s32[16,4]{0,1:T(4,128)S(1)}, s32[16,4]{0,1:T(4,128)}, u32[]{:S(2)}) copy-start(s32[16,4]{0,1:T(4,128)} %param.31) | copy-start | bytes 772
  125.8 59.5 %copy-start.8 = (bf16[16,4]{0,1:T(4,128)(2,1)S(1)}, bf16[16,4]{0,1:T(4,128)(2,1)}, u32[]{:S(2)}) copy-start(bf16[16,4]{0,1:T(4,128)(2,1)} %param.32) | copy-start | bytes 388
  173.4 20.4 %copy-start.7 = (bf16[2048]{0:T(1024)(128)(2,1)S(1)}, bf16[2048]{0:T(1024)(128)(2,1)}, u32[]{:S(2)}) copy-start(bf16[2048]{0:T(1024)(128)(2,1)} %param.39) | copy-start | bytes 12292
  187.7 19.0 %all-to-all-start.2 = ((bf16[64,2,2048]{2,1,0:T(2,128)(2,1)}), bf16[64,2,2048]{2,1,0:T(2,128)(2,1)S(1)}, u32[]{:S(2)}, u32[]{:S(2)}) async-start(bf16[64,2,2048]{2,1,0:T(2,128)(2,1)} %reshape.197), calls=%async_computation.2 | async-start | bytes 1048576 | tf_op jit(solution)/shard_map/all_to_all | solution.py:168
  212.6 52.8 %all-to-all-start.3 = ((bf16[64,2,2048]{2,1,0:T(2,128)(2,1)}), bf16[64,2,2048]{2,1,0:T(2,128)(2,1)S(1)}, u32[]{:S(2)}, u32[]{:S(2)}) async-start(bf16[64,2,2048]{2,1,0:T(2,128)(2,1)} %copy.47), calls=%async_computation.3 | async-start | bytes 1048576 | tf_op jit(solution)/shard_map/all_to_all | solution.py:177
  217.4 41.2 %copy-start.4 = (bf16[32,2048]{1,0:T(8,128)(2,1)S(1)}, bf16[32,2048]{1,0:T(8,128)(2,1)}, u32[]{:S(2)}) copy-start(bf16[32,2048]{1,0:T(8,128)(2,1)} %param.38) | copy-start | bytes 393220
  217.4 41.2 %copy-start.5 = (bf16[2048,32]{0,1:T(8,128)(2,1)S(1)}, bf16[2048,32]{0,1:T(8,128)(2,1)}, u32[]{:S(2)}) copy-start(bf16[2048,32]{0,1:T(8,128)(2,1)} %param.37) | copy-start | bytes 393220
  253.8 3.7 %copy-start.1 = (bf16[1024,2048]{1,0:T(8,128)(2,1)S(1)}, bf16[1024,2048]{1,0:T(8,128)(2,1)}, u32[]{:S(2)}) copy-start(bf16[1024,2048]{1,0:T(8,128)(2,1)} %all-gather.8.cloned.1.call-done) | copy-start | bytes 12582916
  265.4 57.4 %all-to-all-start.1 = ((bf16[64,16,2048]{2,1,0:T(8,128)(2,1)}), bf16[64,16,2048]{2,1,0:T(8,128)(2,1)}, u32[]{:S(2)}, u32[]{:S(2)}) async-start(bf16[64,16,2048]{2,1,0:T(8,128)(2,1)} %bitcast.86), calls=%async_computation.1 | async-start | bytes 8388608 | tf_op jit(solution)/shard_map/all_to_all | solution.py:37
Sparse Core Ops, SparseCore 0:
  11.3 93.9 all-gather.3
  108.1 65.2 all-gather.5
  184.6 69.0 all-gather.7
where the time goes:
time: 341 us
  waiting for transfers between devices  239 us (70%)
  matrix products  34.9 us (10%)
  starting transfers between devices  17.9 us (5%)
  other arithmetic  15.6 us (5%)
  between operations  14.1 us (4%)
  blocking collectives  13.2 us (4%)
  local copies, waits for them, and re-layouts  6 us (2%)
    all_gather x1, waiting for transfers between devices, in_one_piece(): out, at, done = (lax.all_gather(both, axis, axis=dim, tiled=True), 0, [])  91.6 us
    all_to_all x1, waiting for transfers between devices, summed_on_arrival(): tiles = lax.all_to_all(split_up(array, dim, size), axis, 0, 0, tiled=True)  50.4 us
    all_gather x1, waiting for transfers between devices, on_device(): lax.all_gather(w_out, 'ep', axis=1, tiled=True)  47.2 us
    all_gather x1, waiting for transfers between devices, on_device(): segment = lax.all_gather(normed_ffn, 'ep', axis=0, tiled=True)  36.3 us
    all_to_all x2, blocking collectives, sent_to_all(): return lax.all_to_all(copies, axis, split_axis=0, concat_axis=0, tiled=True)  13.2 us
    all_to_all x1, waiting for transfers between devices, on_device(): lax.all_to_all(outgoing, 'ep', split_axis=0, concat_axis=0, tiled=True)  12.9 us
    dot_general x3, matrix products, on_device(): jnp.dot(normed, weight_rows, preferred_element_type=jnp.float32)  7.44 us
  transfers between devices with their start and end apart: 6, of which 5 were waited for; matrix products, arithmetic and copies ran while one was open for 13% of the time, Pallas kernels for 0%

commit v1 on v0

--- a/solution.py
+++ b/solution.py
@@ -145,7 +145,9 @@
     )
     partial_rows = jnp.dot(
         retained,
-        lax.all_gather(w_out, "ep", axis=1, tiled=True),
+        jnp.concatenate(
+            lax.all_to_all(jnp.stack([w_out] * lax.axis_size("ep")), "ep", 0, 0), axis=1
+        ),
         preferred_element_type=jnp.float32,
     )
     rounded = lax.optimization_barrier(partial_rows.astype(jnp.bfloat16)).astype(jnp.float32)

time: 341 us -> 325 us (0.953)
  waiting for transfers between devices: 239 us -> 210 us
  starting transfers between devices: 17.9 us -> 32.2 us
  other arithmetic: 15.6 us -> 12 us
    all_gather x1 -> x0, waiting for transfers between devices: 47.2 us -> none  [on_device(): lax.all_gather(w_out, 'ep', axis=1, tiled=True)]
    all_gather x1, waiting for transfers between devices: 91.6 us -> 110 us  [in_one_piece(): out, at, done = (lax.all_gather(both, axis, axis=dim, tiled=True), 0, [])]
    all_to_all x0 -> x1, starting transfers between devices: none -> 12.2 us  [on_device(): lax.all_to_all(jnp.stack([w_out] * lax.axis_size('ep')), 'ep', 0, 0)]
  transfers between devices with their start and end apart: 6 -> 6, of which waited for: 5 -> 4; matrix products, arithmetic and copies ran while one was open for 13% -> 13% of each run, Pallas kernels for 0% -> 0%
where the time goes in v1:
time: 325 us; the launch traced here: 324 us
  waiting for transfers between devices  210 us (65%)
  matrix products  34.8 us (11%)
  starting transfers between devices  32.2 us (10%)
  between operations  14.5 us (4%)
  other arithmetic  12 us (4%)
  blocking collectives  11.8 us (4%)
  local copies, waits for them, and re-layouts  8.9 us (3%)
    all_gather x1, waiting for transfers between devices, in_one_piece(): out, at, done = (lax.all_gather(both, axis, axis=dim, tiled=True), 0, [])  110 us
    all_to_all x1, waiting for transfers between devices, summed_on_arrival(): tiles = lax.all_to_all(split_up(array, dim, size), axis, 0, 0, tiled=True)  50.4 us
    all_gather x1, waiting for transfers between devices, on_device(): segment = lax.all_gather(normed_ffn, 'ep', axis=0, tiled=True)  37.1 us
    all_to_all x1, waiting for transfers between devices, on_device(): lax.all_to_all(outgoing, 'ep', split_axis=0, concat_axis=0, tiled=True)  12.7 us
    all_to_all x1, starting transfers between devices, on_device(): lax.all_to_all(jnp.stack([w_out] * lax.axis_size('ep')), 'ep', 0, 0)  12.2 us
    all_to_all x2, blocking collectives, sent_to_all(): return lax.all_to_all(copies, axis, split_axis=0, concat_axis=0, tiled=True)  11.8 us
    all_to_all x1, starting transfers between devices, on_device(): lax.all_to_all(outgoing, 'ep', split_axis=0, concat_axis=0, tiled=True)  8.5 us
    dot_general x3, matrix products, on_device(): jnp.dot(normed, weight_rows, preferred_element_type=jnp.float32)  7.36 us
  transfers between devices with their start and end apart: 6, of which 4 were waited for; matrix products, arithmetic and copies ran while one was open for 13% of the time, Pallas kernels for 0%

profile of v1, /device:TPU:1, one launch (start us, length us, event | category | flops | bytes accessed | tf_op | source)
XLA Modules:
  0.0 324.0 jit_solution(8663117152856904478)
XLA Ops:
  7.2 1.7 pad_maximum_fusion
  9.0 2.9 stack.2
  11.9 12.2 %all-to-all-start = ((bf16[64,768,32]{1,2,0:T(8,128)(2,1)}), bf16[64,768,32]{1,2,0:T(8,128)(2,1)}, u32[]{:S(2)}, u32[]{:S(2)}) async-start(bf16[64,768,32]{1,2,0:T(8,128)(2,1)} %stack.2), calls=%async_computation | async-start | bytes 6291456 | tf_op jit(solution)/shard_map/all_to_all | solution.py:149
  24.2 0.1 dynamic-slice_exponential_fusion
  24.3 0.1 fusion.64
  24.5 0.1 multiply_cosine_fusion
  24.6 109.6 %all-gather.3.cloned.1.call-done = bf16[2048,3072]{1,0:T(8,128)(2,1)} async-done(((bf16[32,3072]{1,0:T(8,128)(2,1)}), bf16[2048,3072]{1,0:T(8,128)(2,1)}) %all-gather.3.cloned.1.call-update) | async-done | bytes 12582928 | tf_op jit(solution)/shard_map/all_gather | solution.py:13
  134.2 2.4 fusion.45
  136.7 2.4 fusion.39
  139.2 2.5 fusion.33
  141.7 0.1 multiply_subtract_fusion.1
  141.8 0.1 maximum_bitcast_fusion
  141.9 0.1 maximum_multiply_fusion
  141.9 4.5 %multiply_add_fusion = f32[16,6,128,128]{3,2,1,0:T(8,128)S(1)} fusion(f32[16,6,128,128]{3,2,1,0:T(8,128)} %param.22, f32[16,6,128]{2,1,0:T(8,128)S(1)} %reshape.217, f32[16,6,128]{2,1,0:T(8,128)S(1)} %maximum_multiply_fusion, f32[6]{0:T(128)S(1)} %dynamic-slice_exponential_fusion), kind=kLoop, calls=%fused_computation.2 | loop fusion | flops 4718592 | bytes 12681240 | tf_op jit(solution)/shard_map/add | solution.py:80
  146.4 2.7 copy-done.2
  149.1 5.5 %fusion.84 = f32[16,6,1,128]{3,2,1,0:T(1,128)S(1)} fusion(f32[16,6,128,128]{3,2,1,0:T(8,128)S(1)} %multiply_add_fusion, f32[16,6,128,1]{2,1,0,3:T(8,128)S(1)} %maximum_bitcast_fusion), kind=kOutput, calls=%fused_computation.80 | convolution fusion | flops 18874368 | bytes 6389760 | tf_op jit(solution)/shard_map/shd,shdv->shv/dot_general | solution.py:83
  154.6 0.1 bitcast_reduce_fusion
  154.7 0.2 fusion.80
  154.9 0.1 fusion.81
  155.0 4.5 %convolution_convert_fusion.2 = bf16[16,2048]{1,0:T(8,128)(2,1)S(1)} fusion(bf16[768,2048]{0,1:T(8,128)(2,1)} %bitcast.4, f32[2,8,6,128]{3,2,1,0:T(8,128)S(1)} %bitcast.90, bf16[2048,3072]{1,0:T(8,128)(2,1)} %all-gather.3.cloned.1.call-done, bf16[16,2048]{1,0:T(8,128)(2,1)S(1)} %copy-done.3, f32[2048]{0:T(1024)S(1)} %convert_element_type.100, ...), kind=kOutput, calls=%fused_computation.15 | convolution fusion | flops 100925440 | bytes 6479936 | tf_op jit(solution)/shard_map/dot_general | solution.py:146
  159.5 4.3 %all_to_all.30 = bf16[2,16,2048]{2,1,0:T(8,128)(2,1)S(1)} all-to-all(bf16[2,16,2048]{2,1,0:T(8,128)(2,1)S(1)} %broadcast_in_dim.4), channel_id=1, replica_groups=mesh['ep'=64,'tp'=2] {'tp'}, dimensions={0} | all-to-all | bytes 262144 | tf_op jit(solution)/shard_map/all_to_all | solution.py:22
  163.9 0.1 fusion.68
  164.0 0.7 fusion.70
  164.8 0.1 copy.44
  164.9 0.1 eq.31
  165.0 0.1 reduce_window_sum.11
  165.1 0.2 select_reduce_fusion.1
  165.4 0.1 copy.45
  165.5 0.1 convert_reduce_fusion.2
  165.6 1.2 convolution_convert_fusion.1
  166.8 1.1 reshape.207
  167.9 8.5 %all-to-all-start.3 = ((bf16[64,2,2048]{2,1,0:T(2,128)(2,1)}), bf16[64,2,2048]{2,1,0:T(2,128)(2,1)S(1)}, u32[]{:S(2)}, u32[]{:S(2)}) async-start(bf16[64,2,2048]{2,1,0:T(2,128)(2,1)} %reshape.207), calls=%async_computation.3 | async-start | bytes 1048576 | tf_op jit(solution)/shard_map/all_to_all | solution.py:170
  176.5 12.7 %all-to-all-done.3 = bf16[64,2,2048]{2,1,0:T(2,128)(2,1)S(1)} async-done(((bf16[64,2,2048]{2,1,0:T(2,128)(2,1)}), bf16[64,2,2048]{2,1,0:T(2,128)(2,1)S(1)}, u32[]{:S(2)}, u32[]{:S(2)}) %all-to-all-start.3) | async-done | bytes 524320 | tf_op jit(solution)/shard_map/all_to_all | solution.py:170
  189.1 2.0 fusion.14
  191.2 2.5 convolution_convert_fusion
  193.7 1.4 copy.48
  195.1 4.6 %all-to-all-start.4 = ((bf16[64,2,2048]{2,1,0:T(2,128)(2,1)}), bf16[64,2,2048]{2,1,0:T(2,128)(2,1)S(1)}, u32[]{:S(2)}, u32[]{:S(2)}) async-start(bf16[64,2,2048]{2,1,0:T(2,128)(2,1)} %copy.48), calls=%async_computation.4 | async-start | bytes 1048576 | tf_op jit(solution)/shard_map/all_to_all | solution.py:179
  199.7 37.1 %all-gather.5.cloned.1.call-done = bf16[1024,2048]{1,0:T(8,128)(2,1)} async-done(((bf16[16,2048]{1,0:T(8,128)(2,1)}), bf16[1024,2048]{1,0:T(8,128)(2,1)}) %all-gather.5.cloned.1.call-update) | async-done | bytes 4194320 | tf_op jit(solution)/shard_map/all_gather | solution.py:190
  236.8 3.5 %fusion.102 = f32[1,1024]{1,0:T(1,128)S(1)} fusion(bf16[1024,2048]{1,0:T(8,128)(2,1)} %all-gather.5.cloned.1.call-done, bf16[2048,1]{0,1:T(2,128)(2,1)S(1)} %reshape.221), kind=kOutput, calls=%fused_computation.108 | convolution fusion | flops 4194304 | bytes 4202496 | tf_op jit(solution)/shard_map/dot_general | solution.py:195
  240.3 1.3 fusion.101
  241.7 6.7 %multiply_convert_fusion = bf16[1024,2048]{1,0:T(8,128)(2,1)} fusion(bf16[32,2048]{1,0:T(8,128)(2,1)S(1)} %copy-done.4, f32[1024]{0:T(1024)S(1)} %add_divide_fusion, bf16[1024,2048]{1,0:T(8,128)(2,1)} %all-gather.5.cloned.1.call-done, bf16[2048,32]{0,1:T(8,128)(2,1)S(1)} %copy-done.5, f32[1024,32]{0,1:T(8,128)S(1)} %fusion.101), kind=kOutput, calls=%fused_computation.1 | convolution fusion | flops 272826368 | bytes 8785920 | tf_op jit(solution)/shard_map/dot_general | solution.py:197
  248.4 6.8 %all-to-all-start.2 = ((bf16[64,16,2048]{2,1,0:T(8,128)(2,1)}), bf16[64,16,2048]{2,1,0:T(8,128)(2,1)}, u32[]{:S(2)}, u32[]{:S(2)}) async-start(bf16[64,16,2048]{2,1,0:T(8,128)(2,1)} %bitcast.89), calls=%async_computation.2 | async-start | bytes 8388608 | tf_op jit(solution)/shard_map/all_to_all | solution.py:37
  255.2 0.2 reshape.212
  255.4 50.4 %all-to-all-done.2 = bf16[64,16,2048]{2,1,0:T(8,128)(2,1)} async-done(((bf16[64,16,2048]{2,1,0:T(8,128)(2,1)}), bf16[64,16,2048]{2,1,0:T(8,128)(2,1)}, u32[]{:S(2)}, u32[]{:S(2)}) %all-to-all-start.2) | async-done | bytes 4194336 | tf_op jit(solution)/shard_map/all_to_all | solution.py:37
  305.8 2.9 convert_reduce_fusion
  308.7 0.3 fusion.8
  309.0 7.5 %all_to_all.31 = bf16[2,16,2048]{2,1,0:T(8,128)(2,1)S(1)} all-to-all(bf16[2,16,2048]{2,1,0:T(8,128)(2,1)S(1)} %broadcast_in_dim.5), channel_id=1, replica_groups=mesh['ep'=64,'tp'=2] {'tp'}, dimensions={0} | all-to-all | bytes 262144 | tf_op jit(solution)/shard_map/all_to_all | solution.py:22
  316.5 0.7 fusion.71
  (57 shorter events, 0.6 us)
Async XLA Ops:
  7.2 184.0 %copy-start = (bf16[1,512,2048]{2,1,0:T(8,128)(2,1)S(1)}, bf16[1,512,2048]{2,1,0:T(8,128)(2,1)}, u32[]{:S(2)}) copy-start(bf16[1,512,2048]{2,1,0:T(8,128)(2,1)} %param.35) | copy-start | bytes 6291460
  7.2 127.0 %all-gather.3.cloned.1.call-start = ((), (), s32[]{:S(2)}) async-start(), calls=%async_computation.6 | async-start | bytes 12779520 | tf_op jit(solution)/shard_map/all_gather | solution.py:13
  9.0 15.2 %copy-start.13 = (s32[16]{0:T(128)S(1)}, s32[16]{0:T(128)}, u32[]{:S(2)}) copy-start(s32[16]{0:T(128)} %param.21) | copy-start | bytes 196
  9.0 15.2 %copy-start.8 = (bf16[2048]{0:T(1024)(128)(2,1)S(1)}, bf16[2048]{0:T(1024)(128)(2,1)}, u32[]{:S(2)}) copy-start(bf16[2048]{0:T(1024)(128)(2,1)} %param.23) | copy-start | bytes 12292
  9.0 15.2 %copy-start.9 = (bf16[2048]{0:T(1024)(128)(2,1)S(1)}, bf16[2048]{0:T(1024)(128)(2,1)}, u32[]{:S(2)}) copy-start(bf16[2048]{0:T(1024)(128)(2,1)} %param.30) | copy-start | bytes 12292
  9.0 15.3 %copy-start.3 = (bf16[16,2048]{1,0:T(8,128)(2,1)S(1)}, bf16[16,2048]{1,0:T(8,128)(2,1)}, u32[]{:S(2)}) copy-start(bf16[16,2048]{1,0:T(8,128)(2,1)} %param.20) | copy-start | bytes 196612
  9.0 15.5 %copy-start.11 = (bf16[768]{0:T(1024)(128)(2,1)S(1)}, bf16[768]{0:T(1024)(128)(2,1)}, u32[]{:S(2)}) copy-start(bf16[768]{0:T(1024)(128)(2,1)} %param.28) | copy-start | bytes 4612
  11.9 143.1 %all-to-all-start = ((bf16[64,768,32]{1,2,0:T(8,128)(2,1)}), bf16[64,768,32]{1,2,0:T(8,128)(2,1)}, u32[]{:S(2)}, u32[]{:S(2)}) async-start(bf16[64,768,32]{1,2,0:T(8,128)(2,1)} %stack.2), calls=%async_computation | async-start | bytes 6291456 | tf_op jit(solution)/shard_map/all_to_all | solution.py:149
  24.1 212.7 %all-gather.5.cloned.1.call-start = ((), (), s32[]{:S(2)}) async-start(), calls=%async_computation.7 | async-start | bytes 4259840 | tf_op jit(solution)/shard_map/all_gather | solution.py:190
  146.4 2.7 copy-start.2
  154.6 10.2 %copy-start.7 = (s32[16,4]{0,1:T(4,128)S(1)}, s32[16,4]{0,1:T(4,128)}, u32[]{:S(2)}) copy-start(s32[16,4]{0,1:T(4,128)} %param.31) | copy-start | bytes 772
  154.6 10.9 %copy-start.12 = (bf16[16,4]{0,1:T(4,128)(2,1)S(1)}, bf16[16,4]{0,1:T(4,128)(2,1)}, u32[]{:S(2)}) copy-start(bf16[16,4]{0,1:T(4,128)(2,1)} %param.32) | copy-start | bytes 388
  155.0 21.5 %copy-start.10 = (bf16[2048]{0:T(1024)(128)(2,1)S(1)}, bf16[2048]{0:T(1024)(128)(2,1)}, u32[]{:S(2)}) copy-start(bf16[2048]{0:T(1024)(128)(2,1)} %param.39) | copy-start | bytes 12292
  167.9 21.2 %all-to-all-start.3 = ((bf16[64,2,2048]{2,1,0:T(2,128)(2,1)}), bf16[64,2,2048]{2,1,0:T(2,128)(2,1)S(1)}, u32[]{:S(2)}, u32[]{:S(2)}) async-start(bf16[64,2,2048]{2,1,0:T(2,128)(2,1)} %reshape.207), calls=%async_computation.3 | async-start | bytes 1048576 | tf_op jit(solution)/shard_map/all_to_all | solution.py:170
  193.7 46.7 %copy-start.6 = (bf16[2048,32]{0,1:T(8,128)(2,1)S(1)}, bf16[2048,32]{0,1:T(8,128)(2,1)}, u32[]{:S(2)}) copy-start(bf16[2048,32]{0,1:T(8,128)(2,1)} %param.36) | copy-start | bytes 393220
  195.1 53.4 %all-to-all-start.4 = ((bf16[64,2,2048]{2,1,0:T(2,128)(2,1)}), bf16[64,2,2048]{2,1,0:T(2,128)(2,1)S(1)}, u32[]{:S(2)}, u32[]{:S(2)}) async-start(bf16[64,2,2048]{2,1,0:T(2,128)(2,1)} %copy.48), calls=%async_computation.4 | async-start | bytes 1048576 | tf_op jit(solution)/shard_map/all_to_all | solution.py:179
  199.7 42.0 %copy-start.4 = (bf16[32,2048]{1,0:T(8,128)(2,1)S(1)}, bf16[32,2048]{1,0:T(8,128)(2,1)}, u32[]{:S(2)}) copy-start(bf16[32,2048]{1,0:T(8,128)(2,1)} %param.38) | copy-start | bytes 393220
  199.7 42.0 %copy-start.5 = (bf16[2048,32]{0,1:T(8,128)(2,1)S(1)}, bf16[2048,32]{0,1:T(8,128)(2,1)}, u32[]{:S(2)}) copy-start(bf16[2048,32]{0,1:T(8,128)(2,1)} %param.37) | copy-start | bytes 393220
  236.8 3.5 %copy-start.1 = (bf16[1024,2048]{1,0:T(8,128)(2,1)S(1)}, bf16[1024,2048]{1,0:T(8,128)(2,1)}, u32[]{:S(2)}) copy-start(bf16[1024,2048]{1,0:T(8,128)(2,1)} %all-gather.5.cloned.1.call-done) | copy-start | bytes 12582916
  248.4 57.4 %all-to-all-start.2 = ((bf16[64,16,2048]{2,1,0:T(8,128)(2,1)}), bf16[64,16,2048]{2,1,0:T(8,128)(2,1)}, u32[]{:S(2)}, u32[]{:S(2)}) async-start(bf16[64,16,2048]{2,1,0:T(8,128)(2,1)} %bitcast.89), calls=%async_computation.2 | async-start | bytes 8388608 | tf_op jit(solution)/shard_map/all_to_all | solution.py:37
Sparse Core Ops, SparseCore 0:
  11.3 122.8 all-gather.2
  164.9 71.8 all-gather.4
